TPU v7x, 32 devices: a whole 2x2x4 slice. The times are simulated.
32 devices in a mesh: ra: 4 (over z), cb: 2 (over y), dp: 4 (over x, core).
Axes of the slice: x: 2, y: 2, z: 4, core: 2. Of those that a mesh axis runs over, the one named last changes fastest.
Arguments:
- tokens: bfloat16 [1792, 4096], P('dp', 'ra'), may hold values from -70 to 70
- norm_in: bfloat16 [4096], P('ra'), may hold values from 0.099609375 to 1.8984375
- w_up: float32 [4096, 16384], P(None, ('ra', 'cb')), may hold values from -0.09375 to 0.09375
- up_scale: float32 [16384], P(('ra', 'cb')), may hold values from 0.5 to 2
- w_down: float32 [16384, 4096], P('ra', 'cb'), may hold values from -0.0625 to 0.0625
- down_scale: float32 [4096], P('cb'), may hold values from 0.5 to 2
- norm_out: float32 [4096], P('cb'), may hold values from 0.1 to 1.9
Outputs:
- result: bfloat16 [1792, 4096], P('dp', 'cb')
All inputs are finite; a program needn't handle non-finite values.
Results may differ from a plain program's by a relative error of at most 0.024.
Values may be sent and summed in bfloat16 or wider, within the bound.
A program may use at most 128 MiB of HBM per device.

v0:
```python
import jax
import jax.numpy as jnp
from jax import lax
from jax.sharding import PartitionSpec as P

epsilon = 1e-06
resid_weight = 0.25


def per_device(tokens, norm_in, w_up, up_scale, w_down, down_scale, norm_out):
    whole_rows, whole_gain = (
        lax.all_gather(tokens, "ra", axis=1, tiled=True),
        lax.all_gather(norm_in, "ra", axis=0, tiled=True),
    )
    whole_float = whole_rows.astype(jnp.float32)
    model_width = whole_float.shape[1]
    inv_in = lax.rsqrt(jnp.mean(whole_float * whole_float, axis=-1) + epsilon)
    normed = (whole_float * whole_gain.astype(jnp.float32)).astype(jnp.bfloat16)
    pre_act = jnp.dot(normed, w_up.astype(jnp.bfloat16), preferred_element_type=jnp.float32)
    pre_act = pre_act * inv_in[:, None] * up_scale
    hidden = jnp.square(jax.nn.relu(pre_act)).astype(jnp.bfloat16)
    down_bf = w_down.astype(jnp.bfloat16)
    quarter = down_bf.shape[1]
    partial_value = jnp.dot(
        lax.all_gather(hidden, "cb", axis=1, tiled=True),
        down_bf,
        preferred_element_type=jnp.float32,
    )
    col_block = lax.axis_index("cb")
    x_quarter = lax.dynamic_slice_in_dim(whole_float, col_block * quarter, quarter, 1)
    down = lax.psum(partial_value.astype(jnp.bfloat16), "ra").astype(jnp.float32)
    mixed = resid_weight * x_quarter + down * down_scale
    total_sq = lax.psum(jnp.sum(mixed * mixed, axis=-1), "cb")
    inv_out = lax.rsqrt(total_sq / model_width + epsilon)
    return (mixed * inv_out[:, None] * norm_out).astype(jnp.bfloat16)


def solution(mesh):
    placed = (
        P("dp", "ra"),
        P("ra"),
        P(None, ("ra", "cb")),
        P(("ra", "cb")),
        P("ra", "cb"),
        P("cb"),
        P("cb"),
    )
    return jax.shard_map(
        per_device, mesh=mesh, in_specs=placed, out_specs=P("dp", "cb"), check_vma=False
    )
```

profile of v0, /device:TPU:0, one launch (start us, length us, event | category | flops | bytes accessed | tf_op | source)
XLA Modules:
  0.0 266.2 jit_solution(17357724036729051572)
XLA Ops:
  6.5 0.0 copy-start.3
  6.5 0.0 all-gather.3.cloned.1.call-start
  6.5 0.7 all-gather.3.cloned.1.call-update
  7.3 0.0 all-gather.5.cloned.1.call-start
  7.3 13.8 %all_gather.10 = bf16[4096]{0:T(1024)(128)(2,1)S(1)} all-gather(bf16[1024]{0:T(1024)(128)(2,1)} %param.8), channel_id=1, replica_groups=mesh['ra'=4,'cb'=2,'dp'=4] {'ra'}, dimensions={0}, use_global_device_ids=true | all-gather | bytes 10240 | tf_op jit(solution)/shard_map/all_gather | solution.py:13
  21.1 62.7 %all-gather.3.cloned.1.call-done = bf16[448,4096]{1,0:T(8,128)(2,1)} async-done(((bf16[448,1024]{1,0:T(8,128)(2,1)}), bf16[448,4096]{1,0:T(8,128)(2,1)}) %all-gather.3.cloned.1.call-update) | async-done | bytes 3670032 | tf_op jit(solution)/shard_map/all_gather | solution.py:12
  83.7 2.8 %multiply_reduce_fusion = f32[448]{0:T(512)S(1)} fusion(bf16[448,4096]{1,0:T(8,128)(2,1)} %all-gather.3.cloned.1.call-done), kind=kLoop, calls=%fused_computation.4 | loop fusion | flops 5504576 | bytes 3671808 | tf_op jit(solution)/shard_map/reduce_sum | solution.py:17
  86.6 0.0 copy-done.3
  86.6 16.5 %multiply_convert_fusion.3 = bf16[448,2048]{1,0:T(8,128)(2,1)} fusion(f32[4096,2048]{1,0:T(8,128)} %param.9, f32[4096]{0:T(1024)S(1)} %convert_element_type.28, bf16[448,4096]{1,0:T(8,128)(2,1)} %all-gather.3.cloned.1.call-done, f32[2048]{0:T(1024)S(1)} %copy-done.3, f32[448]{0:T(512)S(1)} %add_rsqrt_fusion.1), kind=kOutput, calls=%fused_computation.9 | convolution fusion | flops 7534673920 | bytes 39085824 | tf_op jit(solution)/shard_map/dot_general | solution.py:19
  103.1 0.0 all-gather.5.cloned.1.call-update
  103.2 0.0 all-reduce.2.cloned.1.call-start
  103.2 49.5 %all-gather.5.cloned.1.call-done = bf16[448,4096]{1,0:T(8,128)(2,1)} async-done(((bf16[448,2048]{1,0:T(8,128)(2,1)}), bf16[448,4096]{1,0:T(8,128)(2,1)}) %all-gather.5.cloned.1.call-update) | async-done | bytes 3670032 | tf_op jit(solution)/shard_map/all_gather | solution.py:25
  152.7 16.5 %fusion.8 = bf16[448,2048]{1,0:T(8,128)(2,1)} fusion(bf16[448,4096]{1,0:T(8,128)(2,1)} %all-gather.5.cloned.1.call-done, f32[4096,2048]{1,0:T(8,128)} %param.11), kind=kOutput, calls=%fused_computation.12 | convolution fusion | flops 7525498880 | bytes 39059456 | tf_op jit(solution)/shard_map/dot_general | solution.py:24
  169.2 0.0 all-reduce.2.cloned.1.call-update
  169.2 0.0 copy-start.1
  169.2 5.9 %convert_element_type.27 = f32[448,4096]{1,0:T(8,128)} convert(bf16[448,4096]{1,0:T(8,128)(2,1)} %all-gather.3.cloned.1.call-done) | non-fusion elementwise | flops 1835008 | bytes 11010048 | tf_op jit(solution)/shard_map/convert_element_type | solution.py:15
  175.1 0.0 copy-start.2
  175.1 71.8 %all-reduce.2.cloned.1.call-done = bf16[448,2048]{1,0:T(8,128)(2,1)} async-done(((bf16[448,2048]{1,0:T(8,128)(2,1)}), bf16[448,2048]{1,0:T(8,128)(2,1)}) %all-reduce.2.cloned.1.call-update) | async-done | bytes 1835024 | tf_op jit(solution)/shard_map/psum | solution.py:31
  247.0 0.0 copy-done.1
  247.0 0.0 copy-start
  247.0 3.5 %multiply_reduce_fusion.1 = f32[448]{0:T(512)S(1)} fusion(bf16[448,2048]{1,0:T(8,128)(2,1)} %all-reduce.2.cloned.1.call-done, f32[448,4096]{1,0:T(8,128)} %convert_element_type.27, s32[]{:T(128)S(6)} %select_n.3, f32[2048]{0:T(1024)S(1)} %copy-done.1), kind=kLoop, calls=%fused_computation.7 | loop fusion | flops 5504576 | bytes 5515012 | tf_op jit(solution)/shard_map/reduce_sum | solution.py:33
  250.5 4.9 %psum.15 = f32[448]{0:T(512)S(1)} all-reduce(f32[448]{0:T(512)S(1)} %multiply_reduce_fusion.1), channel_id=1, replica_groups=mesh['ra'=4,'cb'=2,'dp'=4] {'cb'}, use_global_device_ids=true, to_apply=%region_3.4 | all-reduce | flops 448 | bytes 3584 | tf_op jit(solution)/shard_map/psum | solution.py:33
  255.4 0.0 copy-done.2
  255.4 0.0 copy-done
  255.4 4.2 %multiply_convert_fusion.2 = bf16[448,2048]{1,0:T(8,128)(2,1)} fusion(bf16[448,2048]{1,0:T(8,128)(2,1)S(1)} %copy-done, f32[448,4096]{1,0:T(8,128)} %convert_element_type.27, s32[]{:T(128)S(6)} %select_n.3, f32[2048]{0:T(1024)S(1)} %copy-done.2, f32[448]{0:T(512)S(1)} %add_rsqrt_fusion, f32[2048]{0:T(1024)S(1)} %copy-done.1), kind=kLoop, calls=%fused_computation.6 | loop fusion | flops 6422528 | bytes 7358212 | tf_op jit(solution)/shard_map/convert_element_type | solution.py:35
  (3 shorter events, 0.0 us)
Async XLA Ops:
  6.5 80.1 %copy-start.3 = (f32[2048]{0:T(1024)S(1)}, f32[2048]{0:T(1024)}, u32[]{:S(2)}) copy-start(f32[2048]{0:T(1024)} %param.10) | copy-start | bytes 24580
  6.5 77.2 %all-gather.3.cloned.1.call-start = ((), (), s32[]{:S(2)}) async-start(), calls=%async_computation | async-start | bytes 4587520 | tf_op jit(solution)/shard_map/all_gather | solution.py:12
  7.3 145.4 %all-gather.5.cloned.1.call-start = ((), (), s32[]{:S(2)}) async-start(), calls=%async_computation.1 | async-start | bytes 5505024 | tf_op jit(solution)/shard_map/all_gather | solution.py:25
  103.2 143.8 %all-reduce.2.cloned.1.call-start = ((), (), s32[]{:S(2)}) async-start(), calls=%async_computation.2 | async-start | bytes 3670016 | tf_op jit(solution)/shard_map/psum | solution.py:31
  169.2 77.8 %copy-start.1 = (f32[2048]{0:T(1024)S(1)}, f32[2048]{0:T(1024)}, u32[]{:S(2)}) copy-start(f32[2048]{0:T(1024)} %param.12) | copy-start | bytes 24580
  175.1 80.3 %copy-start.2 = (f32[2048]{0:T(1024)S(1)}, f32[2048]{0:T(1024)}, u32[]{:S(2)}) copy-start(f32[2048]{0:T(1024)} %param.13) | copy-start | bytes 24580
  247.0 8.5 %copy-start = (bf16[448,2048]{1,0:T(8,128)(2,1)S(1)}, bf16[448,2048]{1,0:T(8,128)(2,1)}, u32[]{:S(2)}) copy-start(bf16[448,2048]{1,0:T(8,128)(2,1)} %all-reduce.2.cloned.1.call-done) | copy-start | bytes 5505028
Sparse Core Ops, SparseCore 0:
  8.9 74.8 all-gather.2
  103.3 49.3 all-gather.4
  169.3 77.5 all-reduce.1
where the time goes:
time: 266 us
  waiting for transfers between devices  185 us (70%)
  matrix products  33 us (12%)
  blocking collectives  18.7 us (7%)
  other arithmetic  16.5 us (6%)
  between operations  13.1 us (5%)
    psum x1, waiting for transfers between devices, per_device(): lax.psum(partial_value.astype(jnp.bfloat16), 'ra').astype(jnp.float32)  71.8 us
    all_gather x1, waiting for transfers between devices, per_device(): lax.all_gather(tokens, 'ra', axis=1, tiled=True)  62.7 us
    all_gather x1, waiting for transfers between devices, per_device(): lax.all_gather(hidden, 'cb', axis=1, tiled=True)  49.5 us
    dot_general x1, matrix products, per_device(): jnp.dot(normed, w_up.astype(jnp.bfloat16), preferred_element_type=jnp.flo...  16.5 us
    dot_general x1, matrix products, per_device(): jnp.dot(lax.all_gather(hidden, 'cb', axis=1, tiled=True), down_bf, prefer...  16.5 us
    all_gather x1, blocking collectives, per_device(): lax.all_gather(norm_in, 'ra', axis=0, tiled=True)  13.8 us
    convert_element_type x1, other arithmetic, per_device(): whole_float = whole_rows.astype(jnp.float32)  5.91 us
  transfers between devices with their start and end apart: 3, of which 3 were waited for; matrix products, arithmetic and copies ran while one was open for 2% of the time, Pallas kernels for 0%

commit v1 on v0

--- a/solution.py
+++ b/solution.py
@@ -28,7 +28,7 @@
     )
     col_block = lax.axis_index("cb")
     x_quarter = lax.dynamic_slice_in_dim(whole_float, col_block * quarter, quarter, 1)
-    down = lax.psum(partial_value.astype(jnp.bfloat16), "ra").astype(jnp.float32)
+    down = lax.all_gather(partial_value.astype(jnp.bfloat16), "ra").sum(axis=0).astype(jnp.float32)
     mixed = resid_weight * x_quarter + down * down_scale
     total_sq = lax.psum(jnp.sum(mixed * mixed, axis=-1), "cb")
     inv_out = lax.rsqrt(total_sq / model_width + epsilon)

time: 266 us -> 326 us (1.23)
  waiting for transfers between devices: 185 us -> 240 us
  other arithmetic: 16.5 us -> 20.7 us
    all_gather x0 -> x1, waiting for transfers between devices: none -> 127 us  [per_device(): lax.all_gather(partial_value.astype(jnp.bfloat16), 'ra').sum(axis=0)]
    psum x1 -> x0, waiting for transfers between devices: 71.8 us -> none  [per_device(): lax.psum(partial_value.astype(jnp.bfloat16), 'ra').astype(jnp.float32)]
    reduce_sum x0 -> x1, other arithmetic: none -> 4.88 us  [per_device(): lax.all_gather(partial_value.astype(jnp.bfloat16), 'ra').sum(axis=0)]
where the time goes in v1:
time: 326 us; the launch traced here: 325 us
  waiting for transfers between devices  240 us (74%)
  matrix products  33 us (10%)
  other arithmetic  20.7 us (6%)
  blocking collectives  18.7 us (6%)
  between operations  13.1 us (4%)
    all_gather x1, waiting for transfers between devices, per_device(): lax.all_gather(partial_value.astype(jnp.bfloat16), 'ra').sum(axis=0)  127 us
    all_gather x1, waiting for transfers between devices, per_device(): lax.all_gather(tokens, 'ra', axis=1, tiled=True)  62.7 us
    all_gather x1, waiting for transfers between devices, per_device(): lax.all_gather(hidden, 'cb', axis=1, tiled=True)  49.5 us
    dot_general x1, matrix products, per_device(): jnp.dot(normed, w_up.astype(jnp.bfloat16), preferred_element_type=jnp.flo...  16.5 us
    dot_general x1, matrix products, per_device(): jnp.dot(lax.all_gather(hidden, 'cb', axis=1, tiled=True), down_bf, prefer...  16.5 us
    all_gather x1, blocking collectives, per_device(): lax.all_gather(norm_in, 'ra', axis=0, tiled=True)  13.8 us
  transfers between devices with their start and end apart: 3, of which 3 were waited for; matrix products, arithmetic and copies ran while one was open for 2% of the time, Pallas kernels for 0%

profile of v1, /device:TPU:0, one launch (start us, length us, event | category | flops | bytes accessed | tf_op | source)
XLA Modules:
  0.0 325.2 jit_solution(142749960122872238)
XLA Ops:
  6.5 0.0 copy-start.2
  6.5 0.0 all-gather.5.cloned.1.call-start
  6.5 0.7 all-gather.5.cloned.1.call-update
  7.3 0.0 all-gather.7.cloned.1.call-start
  7.3 13.8 %all_gather.16 = bf16[4096]{0:T(1024)(128)(2,1)S(1)} all-gather(bf16[1024]{0:T(1024)(128)(2,1)} %param.8), channel_id=1, replica_groups=mesh['ra'=4,'cb'=2,'dp'=4] {'ra'}, dimensions={0}, use_global_device_ids=true | all-gather | bytes 10240 | tf_op jit(solution)/shard_map/all_gather | solution.py:13
  21.1 62.7 %all-gather.5.cloned.1.call-done = bf16[448,4096]{1,0:T(8,128)(2,1)} async-done(((bf16[448,1024]{1,0:T(8,128)(2,1)}), bf16[448,4096]{1,0:T(8,128)(2,1)}) %all-gather.5.cloned.1.call-update) | async-done | bytes 3670032 | tf_op jit(solution)/shard_map/all_gather | solution.py:12
  83.7 2.8 multiply_reduce_fusion
  86.6 0.0 copy-done.2
  86.6 16.5 %multiply_convert_fusion.3 = bf16[448,2048]{1,0:T(8,128)(2,1)} fusion(f32[4096,2048]{1,0:T(8,128)} %param.9, f32[4096]{0:T(1024)S(1)} %convert_element_type.30, bf16[448,4096]{1,0:T(8,128)(2,1)} %all-gather.5.cloned.1.call-done, f32[2048]{0:T(1024)S(1)} %copy-done.2, f32[448]{0:T(512)S(1)} %add_rsqrt_fusion.1), kind=kOutput, calls=%fused_computation.9 | convolution fusion | flops 7534673920 | bytes 39085824 | tf_op jit(solution)/shard_map/dot_general | solution.py:19
  103.1 0.0 all-gather.7.cloned.1.call-update
  103.2 0.0 all-gather.9.cloned.1.call-start
  103.2 49.5 %all-gather.7.cloned.1.call-done = bf16[448,4096]{1,0:T(8,128)(2,1)} async-done(((bf16[448,2048]{1,0:T(8,128)(2,1)}), bf16[448,4096]{1,0:T(8,128)(2,1)}) %all-gather.7.cloned.1.call-update) | async-done | bytes 3670032 | tf_op jit(solution)/shard_map/all_gather | solution.py:25
  152.7 16.5 %fusion.8 = bf16[448,2048]{1,0:T(8,128)(2,1)} fusion(bf16[448,4096]{1,0:T(8,128)(2,1)} %all-gather.7.cloned.1.call-done, f32[4096,2048]{1,0:T(8,128)} %param.11), kind=kOutput, calls=%fused_computation.12 | convolution fusion | flops 7525498880 | bytes 39059456 | tf_op jit(solution)/shard_map/dot_general | solution.py:24
  169.2 0.0 all-gather.9.cloned.1.call-update
  169.2 6.0 %convert_element_type.29 = f32[448,4096]{1,0:T(8,128)} convert(bf16[448,4096]{1,0:T(8,128)(2,1)} %all-gather.5.cloned.1.call-done) | non-fusion elementwise | flops 1835008 | bytes 11010048 | tf_op jit(solution)/shard_map/convert_element_type | solution.py:15
  175.2 126.7 %all-gather.9.cloned.1.call-done = bf16[1792,2048]{1,0:T(8,128)(2,1)} async-done(((bf16[448,2048]{1,0:T(8,128)(2,1)}), bf16[1792,2048]{1,0:T(8,128)(2,1)}) %all-gather.9.cloned.1.call-update) | async-done | bytes 7340048 | tf_op jit(solution)/shard_map/all_gather | solution.py:31
  301.8 0.0 copy-start
  301.8 4.9 %reduce_sum.31 = bf16[448,2048]{1,0:T(8,128)(2,1)S(1)} reduce(bf16[4,448,2048]{2,1,0:T(8,128)(2,1)} %bitcast.2, bf16[]{:T(256)} %constant.25.clone.1), dimensions={0}, to_apply=%region_1.2 | reduce | flops 2752512 | bytes 9175042 | tf_op jit(solution)/shard_map/reduce_sum | solution.py:31
  306.7 0.0 copy-done
  306.7 0.0 copy-start.1
  306.7 2.8 multiply_reduce_fusion.1
  309.6 4.9 %psum.7 = f32[448]{0:T(512)S(1)} all-reduce(f32[448]{0:T(512)S(1)} %multiply_reduce_fusion.1), channel_id=1, replica_groups=mesh['ra'=4,'cb'=2,'dp'=4] {'cb'}, use_global_device_ids=true, to_apply=%region_3.4 | all-reduce | flops 448 | bytes 3584 | tf_op jit(solution)/shard_map/psum | solution.py:33
  314.5 0.0 copy-done.1
  314.5 4.2 %multiply_convert_fusion.2 = bf16[448,2048]{1,0:T(8,128)(2,1)} fusion(bf16[448,2048]{1,0:T(8,128)(2,1)S(1)} %reduce_sum.31, f32[448,4096]{1,0:T(8,128)} %convert_element_type.29, s32[]{:T(128)S(6)} %select_n.3, f32[2048]{0:T(1024)S(1)} %copy-done.1, f32[448]{0:T(512)S(1)} %add_rsqrt_fusion, f32[2048]{0:T(1024)S(1)} %copy-done), kind=kLoop, calls=%fused_computation.6 | loop fusion | flops 6422528 | bytes 7358212 | tf_op jit(solution)/shard_map/convert_element_type | solution.py:35
  (3 shorter events, 0.0 us)
Async XLA Ops:
  6.5 80.1 %copy-start.2 = (f32[2048]{0:T(1024)S(1)}, f32[2048]{0:T(1024)}, u32[]{:S(2)}) copy-start(f32[2048]{0:T(1024)} %param.10) | copy-start | bytes 24580
  6.5 77.2 %all-gather.5.cloned.1.call-start = ((), (), s32[]{:S(2)}) async-start(), calls=%async_computation | async-start | bytes 4587520 | tf_op jit(solution)/shard_map/all_gather | solution.py:12
  7.3 145.4 %all-gather.7.cloned.1.call-start = ((), (), s32[]{:S(2)}) async-start(), calls=%async_computation.1 | async-start | bytes 5505024 | tf_op jit(solution)/shard_map/all_gather | solution.py:25
  103.2 198.6 %all-gather.9.cloned.1.call-start = ((), (), s32[]{:S(2)}) async-start(), calls=%async_computation.2 | async-start | bytes 9175040 | tf_op jit(solution)/shard_map/all_gather | solution.py:31
  301.8 4.9 %copy-start = (f32[2048]{0:T(1024)S(1)}, f32[2048]{0:T(1024)}, u32[]{:S(2)}) copy-start(f32[2048]{0:T(1024)} %param.12) | copy-start | bytes 24580
  306.7 7.8 %copy-start.1 = (f32[2048]{0:T(1024)S(1)}, f32[2048]{0:T(1024)}, u32[]{:S(2)}) copy-start(f32[2048]{0:T(1024)} %param.13) | copy-start | bytes 24580
Sparse Core Ops, SparseCore 0:
  8.9 74.8 all-gather.4
  103.3 49.3 all-gather.6
  169.3 132.4 all-gather.8

commit v2 on v0

--- a/solution.py
+++ b/solution.py
@@ -22,7 +22,7 @@
     down_bf = w_down.astype(jnp.bfloat16)
     quarter = down_bf.shape[1]
     partial_value = jnp.dot(
-        lax.all_gather(hidden, "cb", axis=1, tiled=True),
+        jnp.concatenate(lax.all_gather(hidden, axis_name="cb"), 1),
         down_bf,
         preferred_element_type=jnp.float32,
     )

time: 266 us -> 274 us (1.030)
  local copies, waits for them, and re-layouts: 0.02 us -> 7.9 us
    all_gather x0 -> x1, local copies, waits for them, and re-layouts: none -> 5.81 us  [per_device(): lax.all_gather(hidden, axis_name='cb')]
where the time goes in v2:
time: 274 us
  waiting for transfers between devices  185 us (68%)
  matrix products  32.6 us (12%)
  blocking collectives  18.7 us (7%)
  other arithmetic  16.5 us (6%)
  between operations  13.1 us (5%)
  local copies, waits for them, and re-layouts  7.9 us (3%)
    psum x1, waiting for transfers between devices, per_device(): lax.psum(partial_value.astype(jnp.bfloat16), 'ra').astype(jnp.float32)  71.8 us
    all_gather x1, waiting for transfers between devices, per_device(): lax.all_gather(tokens, 'ra', axis=1, tiled=True)  62.7 us
    all_gather x1, waiting for transfers between devices, per_device(): lax.all_gather(hidden, axis_name='cb')  49.3 us
    dot_general x1, matrix products, per_device(): jnp.dot(normed, w_up.astype(jnp.bfloat16), preferred_element_type=jnp.flo...  16.5 us
    dot_general x1, matrix products, per_device(): jnp.dot(jnp.concatenate(lax.all_gather(hidden, axis_name='cb'), 1), down_...  16 us
    all_gather x1, blocking collectives, per_device(): lax.all_gather(norm_in, 'ra', axis=0, tiled=True)  13.8 us
    convert_element_type x1, other arithmetic, per_device(): whole_float = whole_rows.astype(jnp.float32)  5.91 us
    all_gather x1, local copies, waits for them, and re-layouts, per_device(): lax.all_gather(hidden, axis_name='cb')  5.81 us
  transfers between devices with their start and end apart: 3, of which 3 were waited for; matrix products, arithmetic and copies ran while one was open for 2% of the time, Pallas kernels for 0%

profile of v2, /device:TPU:0, one launch (start us, length us, event | category | flops | bytes accessed | tf_op | source)
XLA Modules:
  0.0 273.6 jit_solution(14719512042375907088)
XLA Ops:
  6.5 0.0 copy-start.3
  6.5 0.0 all-gather.4.cloned.1.call-start
  6.5 0.7 all-gather.4.cloned.1.call-update
  7.3 0.0 all-gather.6.cloned.1.call-start
  7.3 13.8 %all_gather.13 = bf16[4096]{0:T(1024)(128)(2,1)S(1)} all-gather(bf16[1024]{0:T(1024)(128)(2,1)} %param.8), channel_id=1, replica_groups=mesh['ra'=4,'cb'=2,'dp'=4] {'ra'}, dimensions={0}, use_global_device_ids=true | all-gather | bytes 10240 | tf_op jit(solution)/shard_map/all_gather | solution.py:13
  21.1 62.7 %all-gather.4.cloned.1.call-done = bf16[448,4096]{1,0:T(8,128)(2,1)} async-done(((bf16[448,1024]{1,0:T(8,128)(2,1)}), bf16[448,4096]{1,0:T(8,128)(2,1)}) %all-gather.4.cloned.1.call-update) | async-done | bytes 3670032 | tf_op jit(solution)/shard_map/all_gather | solution.py:12
  83.7 2.8 %multiply_reduce_fusion = f32[448]{0:T(512)S(1)} fusion(bf16[448,4096]{1,0:T(8,128)(2,1)} %all-gather.4.cloned.1.call-done), kind=kLoop, calls=%fused_computation.4 | loop fusion | flops 5504576 | bytes 3671808 | tf_op jit(solution)/shard_map/reduce_sum | solution.py:17
  86.6 0.0 copy-done.3
  86.6 16.5 %multiply_convert_fusion.3 = bf16[448,2048]{1,0:T(8,128)(2,1)} fusion(f32[4096,2048]{1,0:T(8,128)} %param.9, f32[4096]{0:T(1024)S(1)} %convert_element_type.28, bf16[448,4096]{1,0:T(8,128)(2,1)} %all-gather.4.cloned.1.call-done, f32[2048]{0:T(1024)S(1)} %copy-done.3, f32[448]{0:T(512)S(1)} %add_rsqrt_fusion.1), kind=kOutput, calls=%fused_computation.9 | convolution fusion | flops 7534673920 | bytes 39085824 | tf_op jit(solution)/shard_map/dot_general | solution.py:19
  103.1 0.0 all-gather.6.cloned.1.call-update
  103.2 0.2 all-reduce.2.cloned.1.call-start
  103.4 49.3 %all-gather.6.cloned.1.call-done = bf16[896,2048]{1,0:T(8,128)(2,1)} async-done(((bf16[448,2048]{1,0:T(8,128)(2,1)}), bf16[896,2048]{1,0:T(8,128)(2,1)}) %all-gather.6.cloned.1.call-update) | async-done | bytes 3670032 | tf_op jit(solution)/shard_map/all_gather | solution.py:25
  152.7 5.8 %copy.9 = bf16[2,448,2048]{2,0,1:T(2,128)(2,1)S(1)} copy(bf16[2,448,2048]{2,1,0:T(8,128)(2,1)} %bitcast.6) | data formatting | bytes 7340032 | tf_op jit(solution)/shard_map/all_gather | solution.py:25
  158.5 2.1 copy.10
  160.6 16.0 %fusion.8 = bf16[448,2048]{1,0:T(8,128)(2,1)} fusion(bf16[448,4096]{1,0:T(8,128)(2,1)S(1)} %bitcast.7, f32[4096,2048]{1,0:T(8,128)} %param.11), kind=kOutput, calls=%fused_computation.12 | convolution fusion | flops 7525498880 | bytes 39059456 | tf_op jit(solution)/shard_map/dot_general | solution.py:24
  176.6 0.0 all-reduce.2.cloned.1.call-update
  176.7 0.0 copy-start.1
  176.7 5.9 %convert_element_type.27 = f32[448,4096]{1,0:T(8,128)} convert(bf16[448,4096]{1,0:T(8,128)(2,1)} %all-gather.4.cloned.1.call-done) | non-fusion elementwise | flops 1835008 | bytes 11010048 | tf_op jit(solution)/shard_map/convert_element_type | solution.py:15
  182.6 0.0 copy-start.2
  182.6 71.8 %all-reduce.2.cloned.1.call-done = bf16[448,2048]{1,0:T(8,128)(2,1)} async-done(((bf16[448,2048]{1,0:T(8,128)(2,1)}), bf16[448,2048]{1,0:T(8,128)(2,1)}) %all-reduce.2.cloned.1.call-update) | async-done | bytes 1835024 | tf_op jit(solution)/shard_map/psum | solution.py:31
  254.4 0.0 copy-done.1
  254.4 0.0 copy-start
  254.4 3.5 %multiply_reduce_fusion.1 = f32[448]{0:T(512)S(1)} fusion(bf16[448,2048]{1,0:T(8,128)(2,1)} %all-reduce.2.cloned.1.call-done, f32[448,4096]{1,0:T(8,128)} %convert_element_type.27, s32[]{:T(128)S(6)} %select_n.3, f32[2048]{0:T(1024)S(1)} %copy-done.1), kind=kLoop, calls=%fused_computation.7 | loop fusion | flops 5504576 | bytes 5515012 | tf_op jit(solution)/shard_map/reduce_sum | solution.py:33
  257.9 4.9 %psum.15 = f32[448]{0:T(512)S(1)} all-reduce(f32[448]{0:T(512)S(1)} %multiply_reduce_fusion.1), channel_id=1, replica_groups=mesh['ra'=4,'cb'=2,'dp'=4] {'cb'}, use_global_device_ids=true, to_apply=%region_3.4 | all-reduce | flops 448 | bytes 3584 | tf_op jit(solution)/shard_map/psum | solution.py:33
  262.9 0.0 copy-done.2
  262.9 0.0 copy-done
  262.9 4.2 %multiply_convert_fusion.2 = bf16[448,2048]{1,0:T(8,128)(2,1)} fusion(bf16[448,2048]{1,0:T(8,128)(2,1)S(1)} %copy-done, f32[448,4096]{1,0:T(8,128)} %convert_element_type.27, s32[]{:T(128)S(6)} %select_n.3, f32[2048]{0:T(1024)S(1)} %copy-done.2, f32[448]{0:T(512)S(1)} %add_rsqrt_fusion, f32[2048]{0:T(1024)S(1)} %copy-done.1), kind=kLoop, calls=%fused_computation.6 | loop fusion | flops 6422528 | bytes 7358212 | tf_op jit(solution)/shard_map/convert_element_type | solution.py:35
  (3 shorter events, 0.0 us)
Async XLA Ops:
  6.5 80.1 %copy-start.3 = (f32[2048]{0:T(1024)S(1)}, f32[2048]{0:T(1024)}, u32[]{:S(2)}) copy-start(f32[2048]{0:T(1024)} %param.10) | copy-start | bytes 24580
  6.5 77.2 %all-gather.4.cloned.1.call-start = ((), (), s32[]{:S(2)}) async-start(), calls=%async_computation | async-start | bytes 4587520 | tf_op jit(solution)/shard_map/all_gather | solution.py:12
  7.3 145.4 %all-gather.6.cloned.1.call-start = ((), (), s32[]{:S(2)}) async-start(), calls=%async_computation.2 | async-start | bytes 5505024 | tf_op jit(solution)/shard_map/all_gather | solution.py:25
  103.2 151.3 %all-reduce.2.cloned.1.call-start = ((), (), s32[]{:S(2)}) async-start(), calls=%async_computation.1 | async-start | bytes 3670016 | tf_op jit(solution)/shard_map/psum | solution.py:31
  176.7 77.8 %copy-start.1 = (f32[2048]{0:T(1024)S(1)}, f32[2048]{0:T(1024)}, u32[]{:S(2)}) copy-start(f32[2048]{0:T(1024)} %param.12) | copy-start | bytes 24580
  182.6 80.3 %copy-start.2 = (f32[2048]{0:T(1024)S(1)}, f32[2048]{0:T(1024)}, u32[]{:S(2)}) copy-start(f32[2048]{0:T(1024)} %param.13) | copy-start | bytes 24580
  254.4 8.5 %copy-start = (bf16[448,2048]{1,0:T(8,128)(2,1)S(1)}, bf16[448,2048]{1,0:T(8,128)(2,1)}, u32[]{:S(2)}) copy-start(bf16[448,2048]{1,0:T(8,128)(2,1)} %all-reduce.2.cloned.1.call-done) | copy-start | bytes 5505028
Sparse Core Ops, SparseCore 0:
  8.9 74.8 all-gather.3
  103.3 49.3 all-gather.5
  176.8 77.5 all-reduce.1
